TPU v7x, 32 devices: a whole 2x2x4 slice. The times are simulated.
32 devices in a mesh: gr: 2 (over core), sp: 8 (over z, y), tp: 2 (over x).
Axes of the slice: x: 2, y: 2, z: 4, core: 2. Of those that a mesh axis runs over, the one named last changes fastest.
Arguments:
- tokens: bfloat16 [4, 2048, 2048], P('gr', ('sp', 'tp')), parts along dimension 0, may hold values from -6 to 6
- key_weight: bfloat16 [2048, 1024], P('sp'), may hold values from -0.125 to 0.125
- value_weight: bfloat16 [2048, 1024], P('sp'), may hold values from -0.125 to 0.125
- queries: bfloat16 [4, 1024], P('gr'), parts along dimension 0, may hold values from -6 to 6
- head_offset: float32 [16], replicated, may hold values from -14 to -3.5
- key_bias: bfloat16 [4, 2048, 16], P('gr', ('sp', 'tp')), parts along dimension 0, may hold values from -0.5 to 12.9
Outputs:
- key_cache: bfloat16 [4, 2048, 1024], P('gr', 'sp', 'tp'), parts along dimension 0
- value_cache: bfloat16 [4, 2048, 1024], P('gr', 'sp', 'tp'), parts along dimension 0
- bias_cache: bfloat16 [4, 2048, 16], P('gr', 'sp', 'tp'), parts along dimension 0
- reading: float32 [4, 1024], P('gr', 'tp'), parts along dimension 0
There are 2 independent parts, one for each index of `gr`. A program takes and returns all parts, laid end to end along the dimension named above; an argument that names none is the same for every part. Nothing has to cross between parts.
All inputs are finite; a program needn't handle non-finite values.
Results may differ from a plain program's by a relative error of at most 0.0052.
Values may be sent and summed in bfloat16 or wider, within the bound.
A program may use at most 64 MiB of HBM per device.

v0:
```python
import jax
import jax.numpy as jnp
from jax import lax
from jax.sharding import PartitionSpec as P


def carried_in(x, axis, combine, identity):
    length, position = (lax.axis_size(axis), lax.axis_index(axis))
    everything = lax.all_gather(x, axis)
    start = jnp.broadcast_to(jnp.asarray(identity, x.dtype), x.shape)

    def lap(k, before):
        at = length - 1 - k
        reached = at > position
        new = combine(before, everything[at])
        return jnp.where(reached, new, before)

    return lax.fori_loop(0, length, lap, start)


def add_terms(earlier, later):
    return earlier + later


def normalize(mixture):
    return mixture * lax.rsqrt(jnp.mean(mixture * mixture, axis=-1, keepdims=True) + 1e-06)


def per_device(tokens, key_weight, value_weight, queries, head_offset, key_bias):
    seq_count, pos_dev, model_width = tokens.shape
    head_count = head_offset.shape[0]
    kv_width = key_weight.shape[1]
    head_dim = kv_width // head_count
    score_scale = head_dim ** (-0.5)
    tp_count = lax.axis_size("tp")
    col_width = kv_width // tp_count
    col_start = lax.axis_index("tp") * col_width
    own_cols = jnp.concatenate(
        [
            lax.dynamic_slice_in_dim(key_weight, col_start, col_width, 1),
            lax.dynamic_slice_in_dim(value_weight, col_start, col_width, 1),
        ],
        axis=1,
    )
    full_cols = lax.all_gather(own_cols, "sp", axis=0, tiled=True)
    projected = jnp.einsum(
        "spd,dw->spw",
        lax.all_gather(tokens, "tp", axis=1, tiled=True),
        full_cols,
        preferred_element_type=jnp.float32,
    ).astype(jnp.bfloat16)
    key_cache = projected[:, :, :col_width]
    value_cache = projected[:, :, col_width:]
    bias_cache = lax.all_to_all(key_bias, "tp", split_axis=2, concat_axis=1, tiled=True)
    span_len = key_cache.shape[1]
    local_heads = bias_cache.shape[2]
    key_blocks = key_cache.reshape(seq_count, span_len, local_heads, head_dim)
    value_blocks = value_cache.reshape(seq_count, span_len, local_heads, head_dim)
    query_cols = lax.dynamic_slice_in_dim(queries, col_start, col_width, 1)
    query_heads = query_cols.reshape(seq_count, local_heads, head_dim)
    head_start = lax.axis_index("tp") * local_heads
    local_offset = lax.dynamic_slice_in_dim(head_offset, head_start, local_heads, 0)
    logits = (
        jnp.einsum("sphc,shc->shp", key_blocks, query_heads, preferred_element_type=jnp.float32)
        * score_scale
    )
    logits = (
        logits
        + local_offset[None, :, None]
        + jnp.transpose(bias_cache.astype(jnp.float32), (0, 2, 1))
    )
    fading = jax.nn.log_sigmoid(-logits)
    within = lax.cumsum(fading, axis=2, reverse=True) - fading
    block_total = jnp.sum(fading, axis=2)
    carried = carried_in(block_total, "sp", add_terms, jnp.zeros_like(block_total))
    weights = jnp.exp(jax.nn.log_sigmoid(logits) + within + carried[:, :, None]).astype(
        jnp.bfloat16
    )
    partial_value = jnp.einsum(
        "shp,sphc->shc", weights, value_blocks, preferred_element_type=jnp.float32
    )
    mixture = lax.psum(partial_value, "sp")
    reading = normalize(mixture).reshape(seq_count, col_width)
    return (key_cache, value_cache, bias_cache, reading)


def solution(mesh):
    in_specs = (
        P("gr", ("sp", "tp"), None),
        P("sp", None),
        P("sp", None),
        P("gr", None),
        P(),
        P("gr", ("sp", "tp"), None),
    )
    out_specs = (P("gr", "sp", "tp"), P("gr", "sp", "tp"), P("gr", "sp", "tp"), P("gr", "tp"))
    return jax.shard_map(
        per_device, mesh=mesh, in_specs=in_specs, out_specs=out_specs, check_vma=False
    )
```

profile of v0, /device:TPU:0, one launch (start us, length us, event | category | flops | bytes accessed | tf_op | source)
XLA Modules:
  0.0 179.6 jit_solution(294673093222609058)
XLA Ops:
  7.2 0.7 all-gather.7.cloned.1.call-update
  8.0 1.1 constant_dynamic-slice_fusion.1
  9.1 0.1 copy.28
  9.2 0.1 copy.29
  9.3 0.8 pad_maximum_fusion
  10.2 0.6 copy.20
  10.8 4.2 %all-to-all-start = ((bf16[2,128,16]{1,0,2:T(2,128)(2,1)}), bf16[2,128,16]{1,0,2:T(2,128)(2,1)S(1)}, u32[]{:S(2)}, u32[]{:S(2)}) async-start(bf16[2,128,16]{1,0,2:T(2,128)(2,1)} %copy.20), calls=%async_computation | async-start | bytes 16384 | tf_op jit(solution)/shard_map/all_to_all | solution.py:54
  15.2 30.2 %all-gather.7.cloned.1.call-done = bf16[2,256,2048]{2,1,0:T(8,128)(2,1)} async-done(((bf16[2,128,2048]{2,1,0:T(8,128)(2,1)}), bf16[2,256,2048]{2,1,0:T(8,128)(2,1)}) %all-gather.7.cloned.1.call-update) | async-done | bytes 2097168 | tf_op jit(solution)/shard_map/all_gather | solution.py:48
  45.4 77.3 %all-gather.5.cloned.1.call-done = bf16[2048,1024]{0,1:T(8,128)(2,1)} async-done(((bf16[256,1024]{0,1:T(8,128)(2,1)}), bf16[2048,1024]{0,1:T(8,128)(2,1)}) %all-gather.5.cloned.1.call-update) | async-done | bytes 4194320 | tf_op jit(solution)/shard_map/all_gather | solution.py:45
  122.7 5.2 %fusion.5 = bf16[2,256,1024]{1,2,0:T(8,128)(2,1)S(1)} fusion(bf16[2,256,2048]{2,1,0:T(8,128)(2,1)} %all-gather.7.cloned.1.call-done, bf16[2048,1024]{0,1:T(8,128)(2,1)} %all-gather.5.cloned.1.call-done), kind=kOutput, calls=%fused_computation.4 | convolution fusion | flops 2148007936 | bytes 7340032 | tf_op jit(solution)/shard_map/spd,dw->spw/dot_general | solution.py:46
  128.0 0.2 fusion.19
  128.2 1.0 copy.22
  129.2 0.1 negate_bitcast_fusion
  129.3 0.2 fusion.16
  129.5 17.7 %all-gather.1 = f32[8,2,8]{2,1,0:T(2,128)S(1)} all-gather(f32[1,2,8]{2,1,0:T(2,128)S(1)} %negate_bitcast_fusion.1), channel_id=2, replica_groups=mesh['gr'=2,'sp'=8,'tp'=2] {'sp'}, dimensions={0}, use_global_device_ids=true | all-gather | bytes 576 | tf_op jit(solution)/shard_map/all_gather | solution.py:9
  147.2 0.3 while.16
  147.5 5.0 %reduce-window.6 = f32[2,8,2,128]{3,1,2,0:T(8,128)S(1)} reduce-window(f32[2,8,2,128]{3,1,2,0:T(8,128)S(1)} %get-tuple-element.150, f32[]{:T(128)} %constant.72.clone.1), window={size=1x1x1x128 pad=0_0x0_0x0_0x0_127}, to_apply=%region_0.1 | reduce-window | flops 520192 | bytes 32772 | tf_op jit(solution)/shard_map/reduce-window
  152.5 0.1 slice_reduce_fusion
  152.6 1.0 copy.23
  153.6 0.1 fusion.17
  153.7 0.2 fusion.14
  153.9 17.9 %psum.7 = f32[2,8,64]{2,1,0:T(8,128)S(1)} all-reduce(f32[2,8,64]{2,1,0:T(8,128)S(1)} %bitcast.62), channel_id=1, replica_groups=mesh['gr'=2,'sp'=8,'tp'=2] {'sp'}, use_global_device_ids=true, to_apply=%region_5.6 | all-reduce | flops 1024 | bytes 8192 | tf_op jit(solution)/shard_map/psum | solution.py:82
  171.9 0.1 multiply_reduce_fusion
  172.1 0.7 reshape.53
  (30 shorter events, 0.6 us)
Async XLA Ops:
  7.2 7.9 %copy-start = (bf16[2,1024]{1,0:T(2,128)(2,1)S(1)}, bf16[2,1024]{1,0:T(2,128)(2,1)}, u32[]{:S(2)}) copy-start(bf16[2,1024]{1,0:T(2,128)(2,1)} %param.11) | copy-start | bytes 12292
  7.2 38.2 %all-gather.7.cloned.1.call-start = ((), (), s32[]{:S(2)}) async-start(), calls=%async_computation.2 | async-start | bytes 3145728 | tf_op jit(solution)/shard_map/all_gather | solution.py:48
  7.9 2.3 %copy-start.2 = (bf16[2,128,16]{1,2,0:T(8,128)(2,1)S(1)}, bf16[2,128,16]{1,2,0:T(8,128)(2,1)}, u32[]{:S(2)}) copy-start(bf16[2,128,16]{1,2,0:T(8,128)(2,1)} %param.13) | copy-start | bytes 24580
  7.9 7.2 %copy-start.3 = (f32[16]{0:T(128)S(1)}, f32[16]{0:T(128)}, u32[]{:S(2)}) copy-start(f32[16]{0:T(128)} %param.12) | copy-start | bytes 196
  7.9 114.7 %all-gather.5.cloned.1.call-start = ((), (), s32[]{:S(2)}) async-start(), calls=%async_computation.1 | async-start | bytes 4718592 | tf_op jit(solution)/shard_map/all_gather | solution.py:45
  10.8 118.4 %all-to-all-start = ((bf16[2,128,16]{1,0,2:T(2,128)(2,1)}), bf16[2,128,16]{1,0,2:T(2,128)(2,1)S(1)}, u32[]{:S(2)}, u32[]{:S(2)}) async-start(bf16[2,128,16]{1,0,2:T(2,128)(2,1)} %copy.20), calls=%async_computation | async-start | bytes 16384 | tf_op jit(solution)/shard_map/all_to_all | solution.py:54
  129.3 43.5 %copy-start.1 = (bf16[2,256,8]{1,2,0:T(8,128)(2,1)}, bf16[2,256,8]{1,2,0:T(8,128)(2,1)S(1)}, u32[]{:S(2)}) copy-start(bf16[2,256,8]{1,2,0:T(8,128)(2,1)S(1)} %get-tuple-element.151) | copy-start | bytes 24580
Sparse Core Ops, SparseCore 0:
  9.5 35.8 all-gather.6
  48.0 74.6 all-gather.4
where the time goes:
time: 180 us
  waiting for transfers between devices  108 us (60%)
  blocking collectives  35.7 us (20%)
  between operations  14.2 us (8%)
  other arithmetic  6.49 us (4%)
  matrix products  5.64 us (3%)
  local copies, waits for them, and re-layouts  4.99 us (3%)
  starting transfers between devices  4.31 us (2%)
    all_gather x1, waiting for transfers between devices, per_device(): full_cols = lax.all_gather(own_cols, 'sp', axis=0, tiled=True)  77.3 us
    all_gather x1, waiting for transfers between devices, per_device(): lax.all_gather(tokens, 'tp', axis=1, tiled=True)  30.2 us
    psum x1, blocking collectives, per_device(): mixture = lax.psum(partial_value, 'sp')  17.9 us
    all_gather x1, blocking collectives, carried_in(): everything = lax.all_gather(x, axis)  17.7 us
    dot_general x1, matrix products, per_device(): jnp.einsum('spd,dw->spw', lax.all_gather(tokens, 'tp', axis=1, tiled=True...  5.22 us
    another operation x2, other arithmetic  5.02 us
    all_to_all x1, starting transfers between devices, per_device(): lax.all_to_all(key_bias, 'tp', split_axis=2, concat_axis=1, tiled=True)  4.23 us
  transfers between devices with their start and end apart: 3, of which 2 were waited for; matrix products, arithmetic and copies ran while one was open for 5% of the time, Pallas kernels for 0%

commit v1 on v0

--- a/solution.py
+++ b/solution.py
@@ -27,6 +27,10 @@
 
 
 def per_device(tokens, key_weight, value_weight, queries, head_offset, key_bias):
+
+    def update_notes(message):
+        return jax.lax.all_gather(message, "sp").sum(axis=0)
+
     seq_count, pos_dev, model_width = tokens.shape
     head_count = head_offset.shape[0]
     kv_width = key_weight.shape[1]
@@ -79,7 +83,7 @@
     partial_value = jnp.einsum(
         "shp,sphc->shc", weights, value_blocks, preferred_element_type=jnp.float32
     )
-    mixture = lax.psum(partial_value, "sp")
+    mixture = update_notes(partial_value)
     reading = normalize(mixture).reshape(seq_count, col_width)
     return (key_cache, value_cache, bias_cache, reading)
 

time: 180 us -> 192 us (1.067)
  blocking collectives: 35.7 us -> 48.3 us
    all_gather x0 -> x1, blocking collectives: none -> 30.5 us  [update_notes(): return jax.lax.all_gather(message, 'sp').sum(axis=0)]
    psum x1 -> x0, blocking collectives: 17.9 us -> none  [per_device(): mixture = lax.psum(partial_value, 'sp')]
where the time goes in v1:
time: 192 us
  waiting for transfers between devices  108 us (56%)
  blocking collectives  48.3 us (25%)
  between operations  14.2 us (7%)
  other arithmetic  6.51 us (3%)
  matrix products  5.64 us (3%)
  local copies, waits for them, and re-layouts  4.99 us (3%)
  starting transfers between devices  4.31 us (2%)
    all_gather x1, waiting for transfers between devices, per_device(): full_cols = lax.all_gather(own_cols, 'sp', axis=0, tiled=True)  77.3 us
    all_gather x1, blocking collectives, update_notes(): return jax.lax.all_gather(message, 'sp').sum(axis=0)  30.5 us
    all_gather x1, waiting for transfers between devices, per_device(): lax.all_gather(tokens, 'tp', axis=1, tiled=True)  30.2 us
    all_gather x1, blocking collectives, carried_in(): everything = lax.all_gather(x, axis)  17.7 us
    dot_general x1, matrix products, per_device(): jnp.einsum('spd,dw->spw', lax.all_gather(tokens, 'tp', axis=1, tiled=True...  5.22 us
    another operation x2, other arithmetic  5.02 us
    all_to_all x1, starting transfers between devices, per_device(): lax.all_to_all(key_bias, 'tp', split_axis=2, concat_axis=1, tiled=True)  4.23 us
  transfers between devices with their start and end apart: 3, of which 2 were waited for; matrix products, arithmetic and copies ran while one was open for 5% of the time, Pallas kernels for 0%

profile of v1, /device:TPU:0, one launch (start us, length us, event | category | flops | bytes accessed | tf_op | source)
XLA Modules:
  0.0 192.2 jit_solution(868827216215149373)
XLA Ops:
  7.2 0.7 all-gather.8.cloned.1.call-update
  8.0 1.1 constant_dynamic-slice_fusion.1
  9.1 0.1 copy.28
  9.2 0.1 copy.29
  9.3 0.8 pad_maximum_fusion
  10.2 0.6 copy.20
  10.8 4.2 %all-to-all-start = ((bf16[2,128,16]{1,0,2:T(2,128)(2,1)}), bf16[2,128,16]{1,0,2:T(2,128)(2,1)S(1)}, u32[]{:S(2)}, u32[]{:S(2)}) async-start(bf16[2,128,16]{1,0,2:T(2,128)(2,1)} %copy.20), calls=%async_computation | async-start | bytes 16384 | tf_op jit(solution)/shard_map/all_to_all | solution.py:58
  15.2 30.2 %all-gather.8.cloned.1.call-done = bf16[2,256,2048]{2,1,0:T(8,128)(2,1)} async-done(((bf16[2,128,2048]{2,1,0:T(8,128)(2,1)}), bf16[2,256,2048]{2,1,0:T(8,128)(2,1)}) %all-gather.8.cloned.1.call-update) | async-done | bytes 2097168 | tf_op jit(solution)/shard_map/all_gather | solution.py:52
  45.4 77.3 %all-gather.6.cloned.1.call-done = bf16[2048,1024]{0,1:T(8,128)(2,1)} async-done(((bf16[256,1024]{0,1:T(8,128)(2,1)}), bf16[2048,1024]{0,1:T(8,128)(2,1)}) %all-gather.6.cloned.1.call-update) | async-done | bytes 4194320 | tf_op jit(solution)/shard_map/all_gather | solution.py:49
  122.7 5.2 %fusion.5 = bf16[2,256,1024]{1,2,0:T(8,128)(2,1)S(1)} fusion(bf16[2,256,2048]{2,1,0:T(8,128)(2,1)} %all-gather.8.cloned.1.call-done, bf16[2048,1024]{0,1:T(8,128)(2,1)} %all-gather.6.cloned.1.call-done), kind=kOutput, calls=%fused_computation.4 | convolution fusion | flops 2148007936 | bytes 7340032 | tf_op jit(solution)/shard_map/spd,dw->spw/dot_general | solution.py:50
  128.0 0.2 fusion.19
  128.2 1.0 copy.22
  129.2 0.1 negate_bitcast_fusion
  129.3 0.2 fusion.16
  129.5 17.7 %all-gather.2 = f32[8,2,8]{2,1,0:T(2,128)S(1)} all-gather(f32[1,2,8]{2,1,0:T(2,128)S(1)} %negate_bitcast_fusion.1), channel_id=2, replica_groups=mesh['gr'=2,'sp'=8,'tp'=2] {'sp'}, dimensions={0}, use_global_device_ids=true | all-gather | bytes 576 | tf_op jit(solution)/shard_map/all_gather | solution.py:9
  147.2 0.3 while.16
  147.5 5.0 %reduce-window.6 = f32[2,8,2,128]{3,1,2,0:T(8,128)S(1)} reduce-window(f32[2,8,2,128]{3,1,2,0:T(8,128)S(1)} %get-tuple-element.150, f32[]{:T(128)} %constant.72.clone.1), window={size=1x1x1x128 pad=0_0x0_0x0_0x0_127}, to_apply=%region_0.1 | reduce-window | flops 520192 | bytes 32772 | tf_op jit(solution)/shard_map/reduce-window
  152.5 0.1 slice_reduce_fusion
  152.6 1.0 copy.23
  153.6 0.1 fusion.17
  153.7 0.2 fusion.14
  153.9 30.5 %all-gather.1 = f32[16,8,64]{2,1,0:T(8,128)S(1)} all-gather(f32[2,8,64]{2,1,0:T(8,128)S(1)} %bitcast.64), channel_id=3, replica_groups=mesh['gr'=2,'sp'=8,'tp'=2] {'sp'}, dimensions={0}, use_global_device_ids=true | all-gather | bytes 36864 | tf_op jit(solution)/shard_map/all_gather | solution.py:32
  184.5 0.1 multiply_reduce_fusion
  184.7 0.7 mul.34
  (31 shorter events, 0.6 us)
Async XLA Ops:
  7.2 7.9 %copy-start = (bf16[2,1024]{1,0:T(2,128)(2,1)S(1)}, bf16[2,1024]{1,0:T(2,128)(2,1)}, u32[]{:S(2)}) copy-start(bf16[2,1024]{1,0:T(2,128)(2,1)} %param.11) | copy-start | bytes 12292
  7.2 38.2 %all-gather.8.cloned.1.call-start = ((), (), s32[]{:S(2)}) async-start(), calls=%async_computation.2 | async-start | bytes 3145728 | tf_op jit(solution)/shard_map/all_gather | solution.py:52
  7.9 2.3 %copy-start.2 = (bf16[2,128,16]{1,2,0:T(8,128)(2,1)S(1)}, bf16[2,128,16]{1,2,0:T(8,128)(2,1)}, u32[]{:S(2)}) copy-start(bf16[2,128,16]{1,2,0:T(8,128)(2,1)} %param.13) | copy-start | bytes 24580
  7.9 7.2 %copy-start.3 = (f32[16]{0:T(128)S(1)}, f32[16]{0:T(128)}, u32[]{:S(2)}) copy-start(f32[16]{0:T(128)} %param.12) | copy-start | bytes 196
  7.9 114.7 %all-gather.6.cloned.1.call-start = ((), (), s32[]{:S(2)}) async-start(), calls=%async_computation.1 | async-start | bytes 4718592 | tf_op jit(solution)/shard_map/all_gather | solution.py:49
  10.8 118.4 %all-to-all-start = ((bf16[2,128,16]{1,0,2:T(2,128)(2,1)}), bf16[2,128,16]{1,0,2:T(2,128)(2,1)S(1)}, u32[]{:S(2)}, u32[]{:S(2)}) async-start(bf16[2,128,16]{1,0,2:T(2,128)(2,1)} %copy.20), calls=%async_computation | async-start | bytes 16384 | tf_op jit(solution)/shard_map/all_to_all | solution.py:58
  129.3 56.1 %copy-start.1 = (bf16[2,256,8]{1,2,0:T(8,128)(2,1)}, bf16[2,256,8]{1,2,0:T(8,128)(2,1)S(1)}, u32[]{:S(2)}) copy-start(bf16[2,256,8]{1,2,0:T(8,128)(2,1)S(1)} %get-tuple-element.151) | copy-start | bytes 24580
Sparse Core Ops, SparseCore 0:
  9.5 35.8 all-gather.7
  48.0 74.6 all-gather.5
